TPU v7x, 32 devices: a whole 2x2x4 slice. The times are simulated.
32 devices in a mesh: sp: 8 (over z, y), tp: 4 (over x, core).
Axes of the slice: x: 2, y: 2, z: 4, core: 2. Of those that a mesh axis runs over, the one named last changes fastest.
Arguments:
- resid: bfloat16 [6144, 2048], P(('sp', 'tp')), may hold values from -6 to 6
- query: bfloat16 [6144, 1024], P('sp', 'tp'), may hold values from -6 to 6
- keys: bfloat16 [6144, 1024], P('sp', 'tp'), may hold values from -6 to 6
- values: bfloat16 [6144, 1024], P('sp', 'tp'), may hold values from -6 to 6
- out_gate: bfloat16 [6144, 1024], P(('sp', 'tp')), may hold values from -6 to 6
- forget_pre: float32 [4, 6144], P('tp', 'sp'), may hold values from 0 to 16
- input_pre: float32 [4, 6144], P('tp', 'sp'), may hold values from -4 to 130
- head_gain: float32 [1024], replicated, may hold values from 0.1 to 1.9
- out_proj: bfloat16 [1024, 2048], replicated, may hold values from -0.1875 to 0.1875
- ffn_gain: float32 [2048], replicated, may hold values from 0.1 to 1.9
- routes: int32 [6144, 2], P(('sp', 'tp')), may hold values from 0 to 7, all different within a row; in each aligned block of 96 rows (0 to 95, 96 to 191, ...) at most 48 rows name the same one
- route_scores: float32 [6144, 2], P(('sp', 'tp')), may hold values from 0.1 to 1
- w_gate: bfloat16 [8, 2048, 512], P('sp'), may hold values from -0.125 to 0.125
- w_up: bfloat16 [8, 2048, 512], P('sp'), may hold values from -0.125 to 0.125
- w_down: bfloat16 [8, 512, 2048], P('sp'), may hold values from -0.25 to 0.25
Outputs:
- layer_out: bfloat16 [6144, 2048], P(('sp', 'tp'))
Inputs may be any that keep to these rules, and one draw needn't show every extreme that they name: `routes`: each row names 2 different experts; in each aligned block of 96 rows no expert is named by more than 48 rows, a bound that some block reaches.
All inputs are finite; a program needn't handle non-finite values.
Results may differ from a plain program's by a relative error of at most 0.0095.
Values may be sent and summed in bfloat16 or wider, within the bound.
A program may use at most 128 MiB of HBM per device.

v0:
```python
import jax
import jax.numpy as jnp
from jax import lax
from jax.sharding import PartitionSpec as P

BLOCK = 64
EPS = 1e-06
FLOOR_LOG = -1e30
HIGHEST = lax.Precision.HIGHEST


def prefix(part, axis, combine, identity):
    place = lax.axis_index(axis)
    gathered = jax.tree.map(lambda a: lax.all_gather(a, axis), part)
    state = jax.tree.map(lambda a, e: jnp.zeros_like(a) + jnp.asarray(e, a.dtype), part, identity)

    def one(step, state):
        return combine(
            state, jax.tree.map(lambda a: lax.dynamic_index_in_dim(a, step, 0, False), gathered)
        )

    return lax.fori_loop(0, place, one, state)


def block_pass(query, keys, values, log_forget, log_input, state):
    seq_len, head_width = query.shape
    blocks = seq_len // BLOCK
    key_scale = head_width ** (-0.5)
    causal = jnp.tril(jnp.ones((BLOCK, BLOCK), dtype=bool))

    def block_step(state_in, inputs):
        state_mat, state_vec, max_log = state_in
        q_block, k_block, v_block, forget_blk, input_blk = inputs
        cum_log = jnp.cumsum(forget_blk)
        block_total = cum_log[-1]
        log_mat = jnp.where(
            causal, cum_log[:, None] - cum_log[None, :] + input_blk[None, :], -jnp.inf
        )
        inter_log = cum_log + max_log
        row_max = jnp.maximum(inter_log, jnp.max(log_mat, axis=1))
        weight_mat = jnp.exp(log_mat - row_max[:, None])
        carry_weight = jnp.exp(inter_log - row_max)
        scores = jnp.dot(q_block, k_block.T, preferred_element_type=jnp.float32) * key_scale
        weights_blk = (scores * weight_mat).astype(jnp.bfloat16)
        q_float = q_block.astype(jnp.float32)
        numerator = carry_weight[:, None] * jnp.dot(
            q_float, state_mat, precision=HIGHEST
        ) + jnp.dot(weights_blk, v_block, preferred_element_type=jnp.float32)
        denominator = carry_weight * jnp.dot(q_float, state_vec, precision=HIGHEST) + jnp.sum(
            weights_blk.astype(jnp.float32), axis=1
        )
        log_keep = block_total - cum_log + input_blk
        new_max = jnp.maximum(block_total + max_log, jnp.max(log_keep))
        keep_weight = jnp.exp(log_keep - new_max)
        decay_now = jnp.exp(block_total + max_log - new_max)
        k_float = k_block.astype(jnp.float32) * key_scale
        state_mat = decay_now * state_mat + jnp.dot(
            (k_float * keep_weight[:, None]).T, v_block.astype(jnp.float32), precision=HIGHEST
        )
        state_vec = decay_now * state_vec + jnp.dot(keep_weight, k_float, precision=HIGHEST)
        return ((state_mat, state_vec, new_max), (numerator, denominator, row_max))

    def to_blocks(array_in):
        return array_in.reshape((blocks, BLOCK) + array_in.shape[1:])

    ignored, outputs = lax.scan(
        block_step,
        state,
        (
            to_blocks(query),
            to_blocks(keys),
            to_blocks(values),
            to_blocks(log_forget),
            to_blocks(log_input),
        ),
    )
    numerator, denominator, row_max = outputs
    return (
        numerator.reshape(seq_len, head_width),
        denominator.reshape(seq_len),
        row_max.reshape(seq_len),
    )


def end_state(keys, values, log_forget, log_input):
    head_width = keys.shape[1]
    cum_log = jnp.cumsum(log_forget)
    block_total = cum_log[-1]
    log_keep = block_total - cum_log + log_input
    max_log = jnp.max(log_keep)
    keep_weight = jnp.exp(log_keep - max_log)
    k_float = keys.astype(jnp.float32) * head_width ** (-0.5)
    state_mat = jnp.dot(
        (k_float * keep_weight[:, None]).T, values.astype(jnp.float32), precision=HIGHEST
    )
    state_vec = jnp.dot(keep_weight, k_float, precision=HIGHEST)
    return (state_mat, state_vec, max_log, block_total)


def join_states(earlier, latter):
    old_mat, old_vec, old_max, old_total = earlier
    new_mat, new_vec, new_max, new_total = latter
    joined_max = jnp.maximum(new_total + old_max, new_max)
    keep_old = jnp.exp(new_total + old_max - joined_max)
    keep_new = jnp.exp(new_max - joined_max)
    joined_mat = keep_old[:, None, None] * old_mat + keep_new[:, None, None] * new_mat
    joined_vec = keep_old[:, None] * old_vec + keep_new[:, None] * new_vec
    return (joined_mat, joined_vec, joined_max, old_total + new_total)


def slot_select(expert_ids, expert_count, capacity):
    flat_ids = expert_ids.reshape(-1)
    one_hot = (flat_ids[:, None] == jnp.arange(expert_count, dtype=jnp.int32)[None, :]).astype(
        jnp.int32
    )
    slot_rank = jnp.sum((jnp.cumsum(one_hot, axis=0) - 1) * one_hot, axis=1)
    target = flat_ids * capacity + slot_rank
    return (
        jnp.arange(expert_count * capacity, dtype=jnp.int32)[:, None] == target[None, :]
    ).astype(jnp.bfloat16)


def run_experts(arrived, w_gate, w_up, w_down, sources):
    local_count = w_gate.shape[0]
    grouped = arrived.reshape(sources, local_count, arrived.shape[1], arrived.shape[2])
    gate_pre = jnp.einsum("pesd,edf->pesf", grouped, w_gate, preferred_element_type=jnp.float32)
    up_pre = jnp.einsum("pesd,edf->pesf", grouped, w_up, preferred_element_type=jnp.float32)
    active = (jax.nn.silu(gate_pre) * up_pre).astype(jnp.bfloat16)
    result = jnp.einsum(
        "pesf,efd->pesd", active, w_down, preferred_element_type=jnp.float32
    ).astype(jnp.bfloat16)
    return result.reshape(arrived.shape)


def shards(
    resid,
    query,
    keys,
    values,
    out_gate,
    forget_pre,
    input_pre,
    head_gain,
    out_proj,
    ffn_gain,
    routes,
    route_scores,
    w_gate,
    w_up,
    w_down,
):
    local_heads = forget_pre.shape[0]
    seq_len = query.shape[0]
    head_width = query.shape[1] // local_heads
    log_forget = jax.nn.log_sigmoid(forget_pre)
    q_heads = query.reshape(seq_len, local_heads, head_width)
    k_heads = keys.reshape(seq_len, local_heads, head_width)
    v_heads = values.reshape(seq_len, local_heads, head_width)
    state_mat, state_vec, max_log, totals = jax.vmap(end_state, in_axes=(1, 1, 0, 0))(
        k_heads, v_heads, log_forget, input_pre
    )
    identity = (
        jnp.zeros((local_heads, head_width, head_width), jnp.float32),
        jnp.zeros((local_heads, head_width), jnp.float32),
        jnp.full((local_heads,), FLOOR_LOG, jnp.float32),
        jnp.zeros((local_heads,), jnp.float32),
    )
    carried = prefix((state_mat, state_vec, max_log, totals), "sp", join_states, identity)
    pass_heads = jax.vmap(block_pass, in_axes=(1, 1, 1, 0, 0, 0), out_axes=(1, 1, 1))
    numerator, denominator, row_max = pass_heads(
        q_heads, k_heads, v_heads, log_forget, input_pre, (identity[0], identity[1], identity[2])
    )
    cum_all = jnp.cumsum(log_forget, axis=1).T + carried[2][None, :]
    joined_max = jnp.maximum(row_max, cum_all)
    keep_own = jnp.exp(row_max - joined_max)
    keep_far = jnp.exp(cum_all - joined_max)
    q_float = q_heads.astype(jnp.float32)
    numerator = keep_own[:, :, None] * numerator + keep_far[:, :, None] * jnp.einsum(
        "lhd,hde->lhe", q_float, carried[0], precision=HIGHEST
    )
    denominator = keep_own * denominator + keep_far * jnp.einsum(
        "lhd,hd->lh", q_float, carried[1], precision=HIGHEST
    )
    row_max = joined_max
    hidden = numerator / jnp.maximum(jnp.abs(denominator), jnp.exp(-row_max))[:, :, None]
    cell_rows = hidden.reshape(seq_len, local_heads * head_width).astype(jnp.bfloat16)
    token_rows = lax.all_to_all(cell_rows, "tp", split_axis=0, concat_axis=1, tiled=True)
    cell_float = token_rows.astype(jnp.float32)
    headed = (
        cell_float
        * lax.rsqrt(jnp.mean(cell_float * cell_float, axis=1, keepdims=True) + EPS)
        * head_gain[None, :]
    )
    gated_out = (headed * jax.nn.sigmoid(out_gate.astype(jnp.float32))).astype(jnp.bfloat16)
    after_mix = resid.astype(jnp.float32) + jnp.dot(
        gated_out, out_proj, preferred_element_type=jnp.float32
    )
    normed_rows = (
        after_mix
        * lax.rsqrt(jnp.mean(after_mix * after_mix, axis=1, keepdims=True) + EPS)
        * ffn_gain[None, :]
    ).astype(jnp.bfloat16)
    row_count = normed_rows.shape[0]
    half_rows = row_count // 2
    route_count = routes.shape[1]
    sources = lax.axis_size("sp")
    expert_count = w_gate.shape[0] * sources
    capacity = max(2, 2 * half_rows * route_count // expert_count)
    selects = [
        slot_select(
            routes[half_idx * half_rows : (half_idx + 1) * half_rows], expert_count, capacity
        )
        for half_idx in range(2)
    ]

    def pack_rows(half_idx):
        selection = (
            selects[half_idx].reshape(expert_count * capacity, half_rows, route_count).sum(axis=2)
        )
        packed = jnp.dot(
            selection,
            normed_rows[half_idx * half_rows : (half_idx + 1) * half_rows],
            preferred_element_type=jnp.float32,
        )
        return packed.astype(jnp.bfloat16).reshape(expert_count, capacity, normed_rows.shape[1])

    send_rows = jnp.concatenate([pack_rows(0), pack_rows(1)], axis=1)
    finished = run_experts(
        lax.all_to_all(send_rows, "sp", split_axis=0, concat_axis=0, tiled=True),
        w_gate,
        w_up,
        w_down,
        sources,
    )
    returned = lax.all_to_all(finished, "sp", split_axis=0, concat_axis=0, tiled=True)
    answers = [returned[:, :capacity], returned[:, capacity:]]
    route_weight = route_scores / jnp.sum(route_scores, axis=1, keepdims=True)
    pieces = []
    for half_idx in range(2):
        gathered = lax.dot_general(
            selects[half_idx],
            answers[half_idx].reshape(expert_count * capacity, -1),
            (((0,), (0,)), ((), ())),
            preferred_element_type=jnp.float32,
        )
        weights_half = route_weight[half_idx * half_rows : (half_idx + 1) * half_rows]
        pieces.append(
            jnp.sum(gathered.reshape(half_rows, route_count, -1) * weights_half[:, :, None], axis=1)
        )
    return (after_mix + jnp.concatenate(pieces, axis=0)).astype(jnp.bfloat16)


def solution(mesh):
    placed = (
        P(("sp", "tp"), None),
        P("sp", "tp"),
        P("sp", "tp"),
        P("sp", "tp"),
        P(("sp", "tp"), None),
        P("tp", "sp"),
        P("tp", "sp"),
        P(),
        P(),
        P(),
        P(("sp", "tp"), None),
        P(("sp", "tp"), None),
        P("sp", None, None),
        P("sp", None, None),
        P("sp", None, None),
    )
    return jax.shard_map(
        shards, mesh=mesh, in_specs=placed, out_specs=P(("sp", "tp"), None), check_vma=False
    )
```

profile of v0, /device:TPU:0, one launch (start us, length us, event | category | flops | bytes accessed | tf_op | source)
XLA Modules:
  0.0 429.5 jit_solution(1679653552651287913)
XLA Ops:
  8.8 2.0 fusion.111
  11.4 2.8 fusion.79
  14.4 1.3 dynamic-slice
  15.7 1.3 bitcast_dynamic-update-slice_fusion
  17.1 1.4 dynamic-update-slice.1
  18.5 136.7 %while.38 = (s32[]{:T(128)}, f32[1,256,256]{2,1,0:T(8,128)S(1)}, f32[1,256]{1,0:T(1,128)S(1)}, f32[1]{0:T(128)}, f32[12,1,64,256]{3,2,1,0:T(8,128)}, /*index=5*/...) while((s32[]{:T(128)}, f32[1,256,256]{2,1,0:T(8,128)S(1)}, ...), condition=%wide.region_5.6_spmd.clone, body=%wide.region_0.5_spmd.clone.sunk | while | flops 105678720 | bytes 1283846 | solution.py:66
  19.4 1.2 fusion.154
  24.5 1.6 fusion.158
  26.1 1.3 fusion.157
  28.3 1.6 convolution_add_fusion.4
  30.8 1.2 fusion.154
  35.9 1.6 fusion.158
  37.5 1.3 fusion.157
  39.7 1.5 convolution_add_fusion.4
  42.2 1.2 fusion.154
  47.3 1.6 fusion.158
  48.9 1.3 fusion.157
  51.1 1.6 convolution_add_fusion.4
  53.6 1.2 fusion.154
  58.7 1.6 fusion.158
  60.3 1.3 fusion.157
  62.5 1.6 convolution_add_fusion.4
  65.0 1.2 fusion.154
  70.1 1.6 fusion.158
  71.7 1.3 fusion.157
  73.8 1.6 convolution_add_fusion.4
  76.4 1.2 fusion.154
  81.5 1.6 fusion.158
  83.1 1.3 fusion.157
  85.2 1.6 convolution_add_fusion.4
  87.7 1.2 fusion.154
  92.9 1.6 fusion.158
  94.5 1.3 fusion.157
  96.6 1.6 convolution_add_fusion.4
  104.3 1.6 fusion.158
  105.9 1.3 fusion.157
  108.0 1.6 convolution_add_fusion.4
  115.6 1.6 fusion.158
  117.3 1.3 fusion.157
  119.4 1.6 convolution_add_fusion.4
  127.0 1.6 fusion.158
  128.7 1.3 fusion.157
  130.8 1.6 convolution_add_fusion.4
  138.4 1.6 fusion.158
  140.1 1.3 fusion.157
  142.2 1.6 convolution_add_fusion.4
  149.8 1.6 fusion.158
  151.5 1.3 fusion.157
  153.6 1.6 convolution_add_fusion.4
  155.2 23.8 %all-reduce.4 = (f32[8]{0:T(128)}, f32[8]{0:T(128)}) all-reduce(f32[8]{0:T(128)S(1)} %bitcast_dynamic-update-slice_fusion, f32[8]{0:T(128)S(1)} %dynamic-update-slice.1), channel_id=1, replica_groups=mesh['sp'=8,'tp'=4] {'sp'}, use_global_device_ids=true, to_apply=%add.2 | all-reduce | flops 16 | bytes 128
  180.4 1.4 copy.45
  186.8 16.3 %all-gather.2 = f32[8,1,256]{2,1,0:T(1,128)S(1)} all-gather(f32[1,1,256]{2,1,0:T(1,128)S(1)} %convolution_bitcast_fusion.3), channel_id=3, replica_groups=mesh['sp'=8,'tp'=4] {'sp'}, dimensions={0}, use_global_device_ids=true | all-gather | bytes 9216 | tf_op jit(solution)/shard_map/all_gather | solution.py:14
  206.0 1.6 fusion.78
  207.6 1.9 copy.46
  209.5 3.5 all-to-all-start
  213.4 6.9 %all-to-all-done = bf16[4,192,256]{2,1,0:T(8,128)(2,1)S(1)} async-done(((bf16[4,192,256]{2,1,0:T(8,128)(2,1)}), bf16[4,192,256]{2,1,0:T(8,128)(2,1)S(1)}, u32[]{:S(2)}, u32[]{:S(2)}) %all-to-all-start) | async-done | bytes 393248 | tf_op jit(solution)/shard_map/all_to_all | solution.py:187
  221.5 3.5 multiply_reduce_fusion
  227.1 103.0 %all_to_all.20 = bf16[8,96,2048]{2,1,0:T(8,128)(2,1)S(1)} all-to-all(bf16[8,96,2048]{2,1,0:T(8,128)(2,1)S(1)} %pad_maximum_fusion), channel_id=1, replica_groups=mesh['sp'=8,'tp'=4] {'sp'}, dimensions={0} | all-to-all | bytes 6291456 | tf_op jit(solution)/shard_map/all_to_all | solution.py:229
  330.1 1.7 copy-done.3
  331.8 3.0 fusion.60
  334.9 8.2 %convolution_convert_fusion = bf16[8,96,2048]{2,1,0:T(8,128)(2,1)} fusion(bf16[1,512,2048]{2,1,0:T(8,128)(2,1)S(1)} %copy-done, bf16[8,96,2048]{2,1,0:T(8,128)(2,1)} %copy-done.3, bf16[1,2048,512]{2,1,0:T(8,128)(2,1)} %param.32, f32[8,96,512]{2,1,0:T(8,128)} %fusion.60), kind=kOutput, calls=%fused_computation.78 | convolution fusion | flops 3225157632 | bytes 12058624 | tf_op jit(solution)/shard_map/pesf,efd->pesd/dot_general | solution.py:129
  343.0 4.5 %all-to-all-start.2 = ((bf16[8,96,2048]{2,1,0:T(8,128)(2,1)}), bf16[8,96,2048]{2,1,0:T(8,128)(2,1)}, u32[]{:S(2)}, u32[]{:S(2)}) async-start(bf16[8,96,2048]{2,1,0:T(8,128)(2,1)} %convolution_convert_fusion), calls=%async_computation.2 | async-start | bytes 6291456 | tf_op jit(solution)/shard_map/all_to_all | solution.py:235
  348.1 69.2 %all-to-all-done.2 = bf16[8,96,2048]{2,1,0:T(8,128)(2,1)} async-done(((bf16[8,96,2048]{2,1,0:T(8,128)(2,1)}), bf16[8,96,2048]{2,1,0:T(8,128)(2,1)}, u32[]{:S(2)}, u32[]{:S(2)}) %all-to-all-start.2) | async-done | bytes 3145760 | tf_op jit(solution)/shard_map/all_to_all | solution.py:235
  417.3 2.3 fusion.112
  (258 shorter events, 79.0 us)
Async XLA Ops:
  6.5 328.3 %copy-start = (bf16[1,512,2048]{2,1,0:T(8,128)(2,1)S(1)}, bf16[1,512,2048]{2,1,0:T(8,128)(2,1)}, u32[]{:S(2)}) copy-start(bf16[1,512,2048]{2,1,0:T(8,128)(2,1)} %param.33) | copy-start | bytes 6291460
  6.5 197.2 %all-gather.5.cloned.1.call-start = ((), (), s32[]{:S(2)}) async-start(), calls=%async_computation.3 | async-start | bytes 2359296 | tf_op jit(solution)/shard_map/all_gather | solution.py:14
  8.1 10.4 %copy-start.21 = (f32[6]{0:T(128)}, f32[6]{0:T(128)S(1)}, u32[]{:S(2)}) copy-start(f32[6]{0:T(128)S(1)} %slice_bitcast_fusion) | copy-start | bytes 76
  155.2 26.6 %copy-start.20 = (s32[192,2]{0,1:T(2,128)S(1)}, s32[192,2]{0,1:T(2,128)}, u32[]{:S(2)}) copy-start(s32[192,2]{0,1:T(2,128)} %param.29) | copy-start | bytes 4612
  155.2 30.5 %copy-start.4 = (bf16[12,1,64,256]{3,2,1,0:T(8,128)(2,1)S(1)}, bf16[12,1,64,256]{3,2,1,0:T(8,128)(2,1)}, u32[]{:S(2)}) copy-start(bf16[12,1,64,256]{3,2,1,0:T(8,128)(2,1)} %get-tuple-element.533) | copy-start | bytes 1179652
  182.1 1.1 copy-start.10
  183.1 0.6 copy-start.14
  183.8 19.9 %copy-start.6 = (s32[96,2]{1,0:T(8,128)}, s32[96,2]{1,0:T(8,128)S(1)}, u32[]{:S(2)}) copy-start(s32[96,2]{1,0:T(8,128)S(1)} %copy.55) | copy-start | bytes 2308
  183.9 19.8 %copy-start.12 = (s32[192]{0:T(256)}, s32[192]{0:T(256)S(1)}, u32[]{:S(2)}) copy-start(s32[192]{0:T(256)S(1)} %eq.114) | copy-start | bytes 2308
  184.9 18.8 %copy-start.16 = (s32[192]{0:T(256)}, s32[192]{0:T(256)S(1)}, u32[]{:S(2)}) copy-start(s32[192]{0:T(256)S(1)} %fusion.98) | copy-start | bytes 2308
  203.8 1.0 copy-start.5
  207.6 5.4 %copy-start.7 = (s32[96,2]{1,0:T(8,128)S(1)}, s32[96,2]{1,0:T(8,128)}, u32[]{:S(2)}) copy-start(s32[96,2]{1,0:T(8,128)} %copy-done.6) | copy-start | bytes 2308
  207.6 5.4 %copy-start.8 = (s32[96,2]{1,0:T(8,128)S(1)}, s32[96,2]{1,0:T(8,128)}, u32[]{:S(2)}) copy-start(s32[96,2]{1,0:T(8,128)} %reduce_sum.106) | copy-start | bytes 2308
  207.6 5.4 %copy-start.9 = (s32[96,2]{1,0:T(8,128)S(1)}, s32[96,2]{1,0:T(8,128)}, u32[]{:S(2)}) copy-start(s32[96,2]{1,0:T(8,128)} %multiply_add_fusion.1) | copy-start | bytes 2308
  209.5 10.8 %all-to-all-start = ((bf16[4,192,256]{2,1,0:T(8,128)(2,1)}), bf16[4,192,256]{2,1,0:T(8,128)(2,1)S(1)}, u32[]{:S(2)}, u32[]{:S(2)}) async-start(bf16[4,192,256]{2,1,0:T(8,128)(2,1)} %bitcast.29), calls=%async_computation | async-start | bytes 786432 | tf_op jit(solution)/shard_map/all_to_all | solution.py:187
  213.4 7.3 %copy-start.24 = (bf16[192,1024]{1,0:T(8,128)(2,1)S(1)}, bf16[192,1024]{1,0:T(8,128)(2,1)}, u32[]{:S(2)}) copy-start(bf16[192,1024]{1,0:T(8,128)(2,1)} %param.23) | copy-start | bytes 1179652
  213.4 7.3 %copy-start.25 = (f32[1024]{0:T(1024)S(1)}, f32[1024]{0:T(1024)}, u32[]{:S(2)}) copy-start(f32[1024]{0:T(1024)} %param.26) | copy-start | bytes 12292
  220.3 1.1 copy-start.23
  221.5 3.5 copy-start.18
  224.9 1.2 copy-start.1
  227.1 104.7 %copy-start.22 = (bf16[1,2048,512]{2,1,0:T(8,128)(2,1)S(1)}, bf16[1,2048,512]{2,1,0:T(8,128)(2,1)}, u32[]{:S(2)}) copy-start(bf16[1,2048,512]{2,1,0:T(8,128)(2,1)} %param.31) | copy-start | bytes 6291460
  330.1 1.7 copy-start.3
  343.0 4.5 %copy-start.11 = (s32[192]{0:T(256)S(1)}, s32[192]{0:T(256)}, u32[]{:S(2)}) copy-start(s32[192]{0:T(256)} %copy-done.10) | copy-start | bytes 2308
  343.0 4.5 %copy-start.15 = (s32[192]{0:T(256)S(1)}, s32[192]{0:T(256)}, u32[]{:S(2)}) copy-start(s32[192]{0:T(256)} %copy-done.14) | copy-start | bytes 2308
  343.0 4.7 %copy-start.13 = (s32[192]{0:T(256)S(1)}, s32[192]{0:T(256)}, u32[]{:S(2)}) copy-start(s32[192]{0:T(256)} %copy-done.12) | copy-start | bytes 2308
  343.0 4.7 %copy-start.17 = (s32[192]{0:T(256)S(1)}, s32[192]{0:T(256)}, u32[]{:S(2)}) copy-start(s32[192]{0:T(256)} %copy-done.16) | copy-start | bytes 2308
  343.0 5.0 %copy-start.19 = (f32[192,2]{0,1:T(2,128)S(1)}, f32[192,2]{0,1:T(2,128)}, u32[]{:S(2)}) copy-start(f32[192,2]{0,1:T(2,128)} %param.30) | copy-start | bytes 4612
  343.0 74.3 %all-to-all-start.2 = ((bf16[8,96,2048]{2,1,0:T(8,128)(2,1)}), bf16[8,96,2048]{2,1,0:T(8,128)(2,1)}, u32[]{:S(2)}, u32[]{:S(2)}) async-start(bf16[8,96,2048]{2,1,0:T(8,128)(2,1)} %convolution_convert_fusion), calls=%async_computation.2 | async-start | bytes 6291456 | tf_op jit(solution)/shard_map/all_to_all | solution.py:235
  420.2 1.4 copy-start.2
Sparse Core Ops, SparseCore 0:
  14.3 51.8 all-gather.4
where the time goes:
time: 436 us; the launch traced here: 430 us
  blocking collectives  143 us (33%)
  matrix products  110 us (25%)
  waiting for transfers between devices  76.2 us (17%)
  other arithmetic  35.8 us (8%)
  local copies, waits for them, and re-layouts  27.3 us (6%)
  loops' own time  15.6 us (4%)
  between operations  14 us (3%)
  starting transfers between devices  7.91 us (2%)
    all_to_all x1, blocking collectives, shards(): lax.all_to_all(send_rows, 'sp', split_axis=0, concat_axis=0, tiled=True)  103 us
    all_to_all x1, waiting for transfers between devices, shards(): lax.all_to_all(finished, 'sp', split_axis=0, concat_axis=0, tiled=True)  69.2 us
    unnamed x1, blocking collectives  23.8 us
    dot_general x12, matrix products, block_step(): jnp.dot(keep_weight, k_float, precision=HIGHEST)  18.9 us
    dot_general x12, matrix products, block_step(): jnp.dot(weights_blk, v_block, preferred_element_type=jnp.float32)  18.9 us
    all_gather x1, blocking collectives, prefix(): gathered = jax.tree.map(lambda a: lax.all_gather(a, axis), part)  16.3 us
    another operation x1, loops' own time, block_pass(): lax.scan(block_step, state, (to_blocks(query), to_blocks(keys), to_blocks...  15.6 us
    dot_general x12, matrix products, block_step(): jnp.dot((k_float * keep_weight[:, None]).T, v_block.astype(jnp.float32),...  15.2 us
  transfers between devices with their start and end apart: 3, of which 2 were waited for; matrix products, arithmetic and copies ran while one was open for 31% of the time, Pallas kernels for 0%

commit v1 on v0

--- a/solution.py
+++ b/solution.py
@@ -7,6 +7,29 @@
 EPS = 1e-06
 FLOOR_LOG = -1e30
 HIGHEST = lax.Precision.HIGHEST
+
+
+def split_up(array, dim, size):
+    dims = array.shape
+    blocks = array.reshape(*dims[:dim], size, dims[dim] // size, *dims[dim + 1 :])
+    return jnp.moveaxis(blocks, dim, 0)
+
+
+def laid_out(blocks, dim):
+    blocks = jnp.moveaxis(blocks, 0, dim)
+    lengths = blocks.shape
+    return blocks.reshape(*lengths[:dim], lengths[dim] * lengths[dim + 1], *lengths[dim + 2 :])
+
+
+def rotated_exchange(shard, axis, split_dim, concat_dim):
+    size, index = (lax.axis_size(axis), lax.axis_index(axis))
+    blocks = split_up(shard, split_dim, size)
+    finished = [blocks[index]]
+    for hop in range(1, size):
+        sent = blocks[(index + hop) % size]
+        finished.append(lax.ppermute(sent, axis, [(i, (i + hop) % size) for i in range(size)]))
+    blocks = jnp.stack(finished)[(index - jnp.arange(size)) % size]
+    return laid_out(blocks, concat_dim)
 
 
 def prefix(part, axis, combine, identity):
@@ -225,13 +248,7 @@
         return packed.astype(jnp.bfloat16).reshape(expert_count, capacity, normed_rows.shape[1])
 
     send_rows = jnp.concatenate([pack_rows(0), pack_rows(1)], axis=1)
-    finished = run_experts(
-        lax.all_to_all(send_rows, "sp", split_axis=0, concat_axis=0, tiled=True),
-        w_gate,
-        w_up,
-        w_down,
-        sources,
-    )
+    finished = run_experts(rotated_exchange(send_rows, "sp", 0, 0), w_gate, w_up, w_down, sources)
     returned = lax.all_to_all(finished, "sp", split_axis=0, concat_axis=0, tiled=True)
     answers = [returned[:, :capacity], returned[:, capacity:]]
     route_weight = route_scores / jnp.sum(route_scores, axis=1, keepdims=True)

time: 436 us -> 443 us (1.016)
  blocking collectives: 143 us -> 40.1 us
  waiting for transfers between devices: 76.2 us -> 128 us
  starting transfers between devices: 7.91 us -> 54.6 us
  local copies, waits for them, and re-layouts: 27.3 us -> 36 us
    all_to_all x1 -> x0, blocking collectives: 103 us -> none  [shards(): lax.all_to_all(send_rows, 'sp', split_axis=0, concat_axis=0, tiled=True)]
    ppermute x0 -> x7, waiting for transfers between devices: none -> 50.3 us  [rotated_exchange(): lax.ppermute(sent, axis, [(i, (i + hop) % size) for i in range(size)])]
    ppermute x0 -> x7, starting transfers between devices: none -> 33.5 us  [rotated_exchange(): lax.ppermute(sent, axis, [(i, (i + hop) % size) for i in range(size)])]
    all_to_all x1, starting transfers between devices: 4.45 us -> 17.5 us  [shards(): lax.all_to_all(finished, 'sp', split_axis=0, concat_axis=0, tiled=True)]
  transfers between devices with their start and end apart: 3 -> 10, of which waited for: 2 -> 6; matrix products, arithmetic and copies ran while one was open for 31% -> 32% of each run, Pallas kernels for 0% -> 0%
where the time goes in v1:
time: 443 us; the launch traced here: 437 us
  waiting for transfers between devices  128 us (29%)
  matrix products  112 us (25%)
  starting transfers between devices  54.6 us (12%)
  blocking collectives  40.1 us (9%)
  other arithmetic  36.4 us (8%)
  local copies, waits for them, and re-layouts  36 us (8%)
  loops' own time  15.8 us (4%)
  between operations  13.9 us (3%)
    all_to_all x1, waiting for transfers between devices, shards(): lax.all_to_all(finished, 'sp', split_axis=0, concat_axis=0, tiled=True)  70.4 us
    ppermute x7, waiting for transfers between devices, rotated_exchange(): lax.ppermute(sent, axis, [(i, (i + hop) % size) for i in range(size)])  50.3 us
    ppermute x7, starting transfers between devices, rotated_exchange(): lax.ppermute(sent, axis, [(i, (i + hop) % size) for i in range(size)])  33.5 us
    unnamed x1, blocking collectives  23.8 us
    dot_general x12, matrix products, block_step(): jnp.dot(keep_weight, k_float, precision=HIGHEST)  18.9 us
    dot_general x12, matrix products, block_step(): jnp.dot(weights_blk, v_block, preferred_element_type=jnp.float32)  18.9 us
    all_to_all x1, starting transfers between devices, shards(): lax.all_to_all(finished, 'sp', split_axis=0, concat_axis=0, tiled=True)  17.5 us
    all_gather x1, blocking collectives, prefix(): gathered = jax.tree.map(lambda a: lax.all_gather(a, axis), part)  16.3 us
  transfers between devices with their start and end apart: 10, of which 6 were waited for; matrix products, arithmetic and copies ran while one was open for 32% of the time, Pallas kernels for 0%

profile of v1, /device:TPU:0, one launch (start us, length us, event | category | flops | bytes accessed | tf_op | source)
XLA Modules:
  0.0 436.9 jit_solution(18399473610555001465)
XLA Ops:
  9.2 1.8 fusion.121
  11.6 2.8 fusion.79
  14.6 1.3 dynamic-slice.11
  17.1 1.3 dynamic-update-slice.1
  18.4 137.1 %while.38 = (s32[]{:T(128)}, f32[1,256,256]{2,1,0:T(8,128)S(1)}, f32[1,256]{1,0:T(1,128)S(1)}, f32[1]{0:T(128)}, f32[12,1,64,256]{3,2,1,0:T(8,128)}, /*index=5*/...) while((s32[]{:T(128)}, f32[1,256,256]{2,1,0:T(8,128)S(1)}, ...), condition=%wide.region_5.6_spmd.clone, body=%wide.region_0.5_spmd.clone.sunk | while | flops 105678720 | bytes 1284879 | solution.py:89
  19.3 1.2 fusion.164
  24.4 1.6 convolution_add_fusion.4
  27.0 1.3 fusion.167
  28.2 1.6 fusion.168
  35.8 1.6 convolution_add_fusion.4
  38.4 1.3 fusion.167
  39.7 1.6 fusion.168
  47.3 1.6 convolution_add_fusion.4
  49.8 1.3 fusion.167
  51.1 1.6 fusion.168
  58.7 1.6 convolution_add_fusion.4
  61.3 1.3 fusion.167
  62.5 1.6 fusion.168
  70.1 1.6 convolution_add_fusion.4
  72.7 1.3 fusion.167
  74.0 1.6 fusion.168
  81.5 1.6 convolution_add_fusion.4
  84.1 1.3 fusion.167
  85.4 1.6 fusion.168
  93.0 1.6 convolution_add_fusion.4
  95.5 1.3 fusion.167
  96.8 1.6 fusion.168
  99.3 1.2 fusion.164
  104.4 1.6 convolution_add_fusion.4
  107.0 1.3 fusion.167
  108.2 1.6 fusion.168
  115.8 1.6 convolution_add_fusion.4
  118.4 1.3 fusion.167
  119.7 1.6 fusion.168
  127.2 1.6 convolution_add_fusion.4
  129.8 1.3 fusion.167
  131.1 1.6 fusion.168
  138.7 1.6 convolution_add_fusion.4
  141.3 1.3 fusion.167
  142.5 1.6 fusion.168
  150.1 1.6 convolution_add_fusion.4
  152.7 1.3 fusion.167
  154.0 1.6 fusion.168
  155.5 23.8 %all-reduce.4 = (f32[8]{0:T(128)}, f32[8]{0:T(128)}) all-reduce(f32[8]{0:T(128)S(1)} %bitcast_dynamic-update-slice_fusion.8, f32[8]{0:T(128)S(1)} %dynamic-update-slice.1), channel_id=1, replica_groups=mesh['sp'=8,'tp'=4] {'sp'}, use_global_device_ids=true, to_apply=%add.2 | all-reduce | flops 16 | bytes 128
  184.7 1.4 copy.45
  188.5 16.3 %all-gather.2 = f32[8,1,256]{2,1,0:T(1,128)S(1)} all-gather(f32[1,1,256]{2,1,0:T(1,128)S(1)} %convolution_bitcast_fusion.3), channel_id=3, replica_groups=mesh['sp'=8,'tp'=4] {'sp'}, dimensions={0}, use_global_device_ids=true | all-gather | bytes 9216 | tf_op jit(solution)/shard_map/all_gather | solution.py:37
  207.6 1.6 fusion.78
  209.2 1.9 copy.46
  211.1 3.6 all-to-all-start
  215.0 7.1 %all-to-all-done = bf16[4,192,256]{2,1,0:T(8,128)(2,1)S(1)} async-done(((bf16[4,192,256]{2,1,0:T(8,128)(2,1)}), bf16[4,192,256]{2,1,0:T(8,128)(2,1)S(1)}, u32[]{:S(2)}, u32[]{:S(2)}) %all-to-all-start) | async-done | bytes 393248 | tf_op jit(solution)/shard_map/all_to_all | solution.py:210
  223.1 3.5 multiply_reduce_fusion
  228.6 5.5 %collective-permute-start = (bf16[1,96,2048]{2,1,0:T(8,128)(2,1)S(1)}, bf16[1,96,2048]{2,1,0:T(8,128)(2,1)S(1)}, u32[]{:S(2)}, u32[]{:S(2)}) collective-permute-start(bf16[1,96,2048]{2,1,0:T(8,128)(2,1)S(1)} %get-tuple-element.296), channel_id=1, source_target_pairs={{0,4},{4,8},{8,12},{12,16},{16,20},{20,24},{24,28},{28,0},{1,5},{5... | collective-permute-start | bytes 1179656 | tf_op jit(solution)/shard_map/ppermute | solution.py:30
  234.1 26.5 %collective-permute-start.5 = (bf16[1,96,2048]{2,1,0:T(8,128)(2,1)S(1)}, bf16[1,96,2048]{2,1,0:T(8,128)(2,1)S(1)}, u32[]{:S(2)}, u32[]{:S(2)}) collective-permute-start(bf16[1,96,2048]{2,1,0:T(8,128)(2,1)S(1)} %fusion.90), channel_id=1, source_target_pairs={{0,24},{4,28},{8,0},{12,4},{16,8},{20,12},{24,16},{28,20},{1,25},{... | collective-permute-start | bytes 1179656 | tf_op jit(solution)/shard_map/ppermute | solution.py:30
  260.6 1.5 collective-permute-start.1
  262.9 7.1 %collective-permute-done = bf16[1,96,2048]{2,1,0:T(8,128)(2,1)S(1)} collective-permute-done((bf16[1,96,2048]{2,1,0:T(8,128)(2,1)S(1)}, bf16[1,96,2048]{2,1,0:T(8,128)(2,1)S(1)}, u32[]{:S(2)}, u32[]{:S(2)}) %collective-permute-start) | collective-permute-done | bytes 393248 | tf_op jit(solution)/shard_map/ppermute | solution.py:30
  270.7 16.8 %collective-permute-done.1 = bf16[1,96,2048]{2,1,0:T(8,128)(2,1)S(1)} collective-permute-done((bf16[1,96,2048]{2,1,0:T(8,128)(2,1)S(1)}, bf16[1,96,2048]{2,1,0:T(8,128)(2,1)S(1)}, u32[]{:S(2)}, u32[]{:S(2)}) %collective-permute-start.1) | collective-permute-done | bytes 393248 | tf_op jit(solution)/shard_map/ppermute | solution.py:30
  288.3 19.3 %collective-permute-done.2 = bf16[1,96,2048]{2,1,0:T(8,128)(2,1)S(1)} collective-permute-done((bf16[1,96,2048]{2,1,0:T(8,128)(2,1)S(1)}, bf16[1,96,2048]{2,1,0:T(8,128)(2,1)S(1)}, u32[]{:S(2)}, u32[]{:S(2)}) %collective-permute-start.2) | collective-permute-done | bytes 393248 | tf_op jit(solution)/shard_map/ppermute | solution.py:30
  308.4 7.2 %collective-permute-done.3 = bf16[1,96,2048]{2,1,0:T(8,128)(2,1)S(1)} collective-permute-done((bf16[1,96,2048]{2,1,0:T(8,128)(2,1)S(1)}, bf16[1,96,2048]{2,1,0:T(8,128)(2,1)S(1)}, u32[]{:S(2)}, u32[]{:S(2)}) %collective-permute-start.3) | collective-permute-done | bytes 393248 | tf_op jit(solution)/shard_map/ppermute | solution.py:30
  318.7 4.3 gather_fusion
  323.0 5.6 %fusion.60 = f32[8,96,512]{2,1,0:T(8,128)} fusion(bf16[8,96,2048]{2,1,0:T(8,128)(2,1)} %gather_fusion, bf16[1,2048,512]{2,1,0:T(8,128)(2,1)} %param.31), kind=kOutput, calls=%fused_computation.104 | convolution fusion | flops 1610612736 | bytes 6815744 | tf_op jit(solution)/shard_map/pesd,edf->pesf/dot_general | solution.py:149
  328.6 8.2 %convolution_convert_fusion = bf16[8,96,2048]{2,1,0:T(8,128)(2,1)} fusion(bf16[1,512,2048]{2,1,0:T(8,128)(2,1)S(1)} %copy-done, bf16[8,96,2048]{2,1,0:T(8,128)(2,1)} %gather_fusion, bf16[1,2048,512]{2,1,0:T(8,128)(2,1)} %param.32, f32[8,96,512]{2,1,0:T(8,128)} %fusion.60), kind=kOutput, calls=%fused_computation.95 | convolution fusion | flops 3225157632 | bytes 12058624 | tf_op jit(solution)/shard_map/pesf,efd->pesd/dot_general | solution.py:152
  336.8 17.5 %all-to-all-start.1 = ((bf16[8,96,2048]{2,1,0:T(8,128)(2,1)}), bf16[8,96,2048]{2,1,0:T(8,128)(2,1)}, u32[]{:S(2)}, u32[]{:S(2)}) async-start(bf16[8,96,2048]{2,1,0:T(8,128)(2,1)} %convolution_convert_fusion), calls=%async_computation.1 | async-start | bytes 6291456 | tf_op jit(solution)/shard_map/all_to_all | solution.py:252
  354.9 70.4 %all-to-all-done.1 = bf16[8,96,2048]{2,1,0:T(8,128)(2,1)} async-done(((bf16[8,96,2048]{2,1,0:T(8,128)(2,1)}), bf16[8,96,2048]{2,1,0:T(8,128)(2,1)}, u32[]{:S(2)}, u32[]{:S(2)}) %all-to-all-start.1) | async-done | bytes 3145760 | tf_op jit(solution)/shard_map/all_to_all | solution.py:252
  425.3 2.3 fusion.122
  (277 shorter events, 93.3 us)
Async XLA Ops:
  6.5 322.1 %copy-start = (bf16[1,512,2048]{2,1,0:T(8,128)(2,1)S(1)}, bf16[1,512,2048]{2,1,0:T(8,128)(2,1)}, u32[]{:S(2)}) copy-start(bf16[1,512,2048]{2,1,0:T(8,128)(2,1)} %param.33) | copy-start | bytes 6291460
  6.5 198.8 %all-gather.5.cloned.1.call-start = ((), (), s32[]{:S(2)}) async-start(), calls=%async_computation.2 | async-start | bytes 2359296 | tf_op jit(solution)/shard_map/all_gather | solution.py:37
  8.1 0.5 copy-start.18
  18.4 161.0 %copy-start.17 = (s32[192,2]{0,1:T(2,128)S(1)}, s32[192,2]{0,1:T(2,128)}, u32[]{:S(2)}) copy-start(s32[192,2]{0,1:T(2,128)} %param.29) | copy-start | bytes 4612
  155.5 32.0 %copy-start.3 = (bf16[12,1,64,256]{3,2,1,0:T(8,128)(2,1)S(1)}, bf16[12,1,64,256]{3,2,1,0:T(8,128)(2,1)}, u32[]{:S(2)}) copy-start(bf16[12,1,64,256]{3,2,1,0:T(8,128)(2,1)} %get-tuple-element.539) | copy-start | bytes 1179652
  179.7 1.0 copy-start.5
  180.7 0.6 copy-start.9
  182.3 1.0 copy-start.7
  183.3 0.6 copy-start.11
  205.4 1.0 copy-start.4
  207.6 7.1 %copy-start.19 = (s32[8]{0:T(128)S(1)}, s32[8]{0:T(128)}, u32[]{:S(2)}) copy-start(s32[8]{0:T(128)} %fusion.116) | copy-start | bytes 100
  207.6 7.1 %copy-start.16 = (s32[96,2]{0,1:T(2,128)S(1)}, s32[96,2]{0,1:T(2,128)}, u32[]{:S(2)}) copy-start(s32[96,2]{0,1:T(2,128)} %copy.51) | copy-start | bytes 2308
  207.6 7.2 %copy-start.15 = (s32[96,2]{0,1:T(2,128)S(1)}, s32[96,2]{0,1:T(2,128)}, u32[]{:S(2)}) copy-start(s32[96,2]{0,1:T(2,128)} %copy.49) | copy-start | bytes 2308
  211.1 11.3 %copy-start.20 = (bf16[192,2048]{1,0:T(8,128)(2,1)S(1)}, bf16[192,2048]{1,0:T(8,128)(2,1)}, u32[]{:S(2)}) copy-start(bf16[192,2048]{1,0:T(8,128)(2,1)} %param.19) | copy-start | bytes 2359300
  211.1 11.3 %copy-start.22 = (f32[1024]{0:T(1024)S(1)}, f32[1024]{0:T(1024)}, u32[]{:S(2)}) copy-start(f32[1024]{0:T(1024)} %param.26) | copy-start | bytes 12292
  211.1 11.0 %all-to-all-start = ((bf16[4,192,256]{2,1,0:T(8,128)(2,1)}), bf16[4,192,256]{2,1,0:T(8,128)(2,1)S(1)}, u32[]{:S(2)}, u32[]{:S(2)}) async-start(bf16[4,192,256]{2,1,0:T(8,128)(2,1)} %bitcast.29), calls=%async_computation | async-start | bytes 786432 | tf_op jit(solution)/shard_map/all_to_all | solution.py:210
  222.1 1.0 copy-start.21
  223.1 3.5 copy-start.13
  226.6 1.2 copy-start.1
  228.6 41.3 %collective-permute-start = (bf16[1,96,2048]{2,1,0:T(8,128)(2,1)S(1)}, bf16[1,96,2048]{2,1,0:T(8,128)(2,1)S(1)}, u32[]{:S(2)}, u32[]{:S(2)}) collective-permute-start(bf16[1,96,2048]{2,1,0:T(8,128)(2,1)S(1)} %get-tuple-element.296), channel_id=1, source_target_pairs={{0,4},{4,8},{8,12},{12,16},{16,20},{20,24},{24,28},{28,0},{1,5},{5... | collective-permute-start | bytes 1179656 | tf_op jit(solution)/shard_map/ppermute | solution.py:30
  234.1 83.0 %collective-permute-start.5 = (bf16[1,96,2048]{2,1,0:T(8,128)(2,1)S(1)}, bf16[1,96,2048]{2,1,0:T(8,128)(2,1)S(1)}, u32[]{:S(2)}, u32[]{:S(2)}) collective-permute-start(bf16[1,96,2048]{2,1,0:T(8,128)(2,1)S(1)} %fusion.90), channel_id=1, source_target_pairs={{0,24},{4,28},{8,0},{12,4},{16,8},{20,12},{24,16},{28,20},{1,25},{... | collective-permute-start | bytes 1179656 | tf_op jit(solution)/shard_map/ppermute | solution.py:30
  260.6 57.3 %collective-permute-start.6 = (bf16[1,96,2048]{2,1,0:T(8,128)(2,1)S(1)}, bf16[1,96,2048]{2,1,0:T(8,128)(2,1)S(1)}, u32[]{:S(2)}, u32[]{:S(2)}) collective-permute-start(bf16[1,96,2048]{2,1,0:T(8,128)(2,1)S(1)} %get-tuple-element.295), channel_id=1, source_target_pairs={{0,28},{4,0},{8,4},{12,8},{16,12},{20,16},{24,20},{28,24},{1,29},{... | collective-permute-start | bytes 1179656 | tf_op jit(solution)/shard_map/ppermute | solution.py:30
  260.6 26.9 %collective-permute-start.1 = (bf16[1,96,2048]{2,1,0:T(8,128)(2,1)S(1)}, bf16[1,96,2048]{2,1,0:T(8,128)(2,1)S(1)}, u32[]{:S(2)}, u32[]{:S(2)}) collective-permute-start(bf16[1,96,2048]{2,1,0:T(8,128)(2,1)S(1)} %get-tuple-element.297), channel_id=1, source_target_pairs={{0,8},{4,12},{8,16},{12,20},{16,24},{20,28},{24,0},{28,4},{1,9},{5... | collective-permute-start | bytes 1179656 | tf_op jit(solution)/shard_map/ppermute | solution.py:30
  262.1 45.5 %collective-permute-start.2 = (bf16[1,96,2048]{2,1,0:T(8,128)(2,1)S(1)}, bf16[1,96,2048]{2,1,0:T(8,128)(2,1)S(1)}, u32[]{:S(2)}, u32[]{:S(2)}) collective-permute-start(bf16[1,96,2048]{2,1,0:T(8,128)(2,1)S(1)} %get-tuple-element.298), channel_id=1, source_target_pairs={{0,12},{4,16},{8,20},{12,24},{16,28},{20,0},{24,4},{28,8},{1,13},{... | collective-permute-start | bytes 1179656 | tf_op jit(solution)/shard_map/ppermute | solution.py:30
  269.9 45.6 %collective-permute-start.3 = (bf16[1,96,2048]{2,1,0:T(8,128)(2,1)S(1)}, bf16[1,96,2048]{2,1,0:T(8,128)(2,1)S(1)}, u32[]{:S(2)}, u32[]{:S(2)}) collective-permute-start(bf16[1,96,2048]{2,1,0:T(8,128)(2,1)S(1)} %get-tuple-element.299), channel_id=1, source_target_pairs={{0,16},{4,20},{8,24},{12,28},{16,0},{20,4},{24,8},{28,12},{1,17},{... | collective-permute-start | bytes 1179656 | tf_op jit(solution)/shard_map/ppermute | solution.py:30
  287.5 28.8 %collective-permute-start.4 = (bf16[1,96,2048]{2,1,0:T(8,128)(2,1)S(1)}, bf16[1,96,2048]{2,1,0:T(8,128)(2,1)S(1)}, u32[]{:S(2)}, u32[]{:S(2)}) collective-permute-start(bf16[1,96,2048]{2,1,0:T(8,128)(2,1)S(1)} %get-tuple-element.300), channel_id=1, source_target_pairs={{0,20},{4,24},{8,28},{12,0},{16,4},{20,8},{24,12},{28,16},{1,21},{... | collective-permute-start | bytes 1179656 | tf_op jit(solution)/shard_map/ppermute | solution.py:30
  336.8 17.6 %copy-start.6 = (s32[192]{0:T(256)S(1)}, s32[192]{0:T(256)}, u32[]{:S(2)}) copy-start(s32[192]{0:T(256)} %copy-done.5) | copy-start | bytes 2308
  336.8 17.6 %copy-start.10 = (s32[192]{0:T(256)S(1)}, s32[192]{0:T(256)}, u32[]{:S(2)}) copy-start(s32[192]{0:T(256)} %copy-done.9) | copy-start | bytes 2308
  336.8 17.8 %copy-start.8 = (s32[192]{0:T(256)S(1)}, s32[192]{0:T(256)}, u32[]{:S(2)}) copy-start(s32[192]{0:T(256)} %copy-done.7) | copy-start | bytes 2308
  336.8 17.8 %copy-start.12 = (s32[192]{0:T(256)S(1)}, s32[192]{0:T(256)}, u32[]{:S(2)}) copy-start(s32[192]{0:T(256)} %copy-done.11) | copy-start | bytes 2308
  336.8 18.0 %copy-start.14 = (f32[192,2]{0,1:T(2,128)S(1)}, f32[192,2]{0,1:T(2,128)}, u32[]{:S(2)}) copy-start(f32[192,2]{0,1:T(2,128)} %param.30) | copy-start | bytes 4612
  336.8 88.5 %all-to-all-start.1 = ((bf16[8,96,2048]{2,1,0:T(8,128)(2,1)}), bf16[8,96,2048]{2,1,0:T(8,128)(2,1)}, u32[]{:S(2)}, u32[]{:S(2)}) async-start(bf16[8,96,2048]{2,1,0:T(8,128)(2,1)} %convolution_convert_fusion), calls=%async_computation.1 | async-start | bytes 6291456 | tf_op jit(solution)/shard_map/all_to_all | solution.py:252
  427.6 1.4 copy-start.2
Sparse Core Ops, SparseCore 0:
  14.5 52.1 all-gather.4
